TPU v7x, 32 devices: a whole 2x2x4 slice. The times are simulated.
32 devices in a mesh: sp: 16 (over z, y, x), tp: 2 (over core).
Axes of the slice: x: 2, y: 2, z: 4, core: 2. Of those that a mesh axis runs over, the one named last changes fastest.
Arguments:
- tokens: bfloat16 [4096, 2048], P('sp'), may hold values from -6 to 6
- query_weight: bfloat16 [2, 2048, 512], P(None, None, 'tp'), may hold values from -0.125 to 0.125
- key_weight: bfloat16 [2, 2048, 512], P(None, None, 'tp'), may hold values from -0.125 to 0.125
- value_weight: bfloat16 [2, 2048, 512], P(None, None, 'tp'), may hold values from -0.125 to 0.125
- out_weight: bfloat16 [2, 512, 2048], replicated, may hold values from -1.5 to 1.5
- rel_table: float32 [2, 8, 257], P(None, 'tp'), may hold values from -5 to 262
- norm_gain: float32 [2, 2048], replicated, may hold values from 0.1 to 1.9
- norm_bias: float32 [2, 2048], replicated, may hold values from -1.5 to 1.5
Outputs:
- encoded: bfloat16 [4096, 2048], P('sp', 'tp')
All inputs are finite; a program needn't handle non-finite values.
Results may differ from a plain program's by a relative error of at most 0.0095.
Values may be sent and summed in bfloat16 or wider, within the bound.
A program may use at most 64 MiB of HBM per device.

v0:
```python
import functools

import jax
import jax.numpy as jnp
from jax import lax
from jax.experimental import pallas as pl
from jax.experimental.pallas import tpu as pltpu
from jax.sharding import PartitionSpec as P

SEG = 64
LEFT = 4
CLIP = 128
LAYERS = 2
LANES = 128

residual_scale = 2.0**0.5
norm_eps = 1e-05
masked_score = -1e30
MESH = pl.DeviceIdType.MESH


def kernel(
    sp_count,
    heads,
    tokens,
    wq_hbm,
    wk_hbm,
    wv_hbm,
    wo_hbm,
    table_hbm,
    gain_hbm,
    shift_hbm,
    out,
    x0,
    x1,
    wq,
    wk,
    wv,
    wo,
    table,
    gain,
    shift,
    query,
    kx,
    vx,
    att,
    total,
    bias,
    padded,
    x_sem,
    w_sem,
    small_sem,
    halo_send,
    halo_recv,
    pair_send,
    pair_recv,
):
    rows, model = x0.shape
    width = query.shape[2]
    head_size = width // heads
    reach = LEFT * SEG
    band = reach + SEG
    segments = rows // SEG
    sp = lax.axis_index("sp")
    tp = lax.axis_index("tp")
    has_next = sp < sp_count - 1
    has_prev = sp > 0
    late = (segments // 2, segments)
    early = (0, segments // 2)

    def w_copy(kind, layer):
        source = (wk_hbm, wv_hbm, wq_hbm, wo_hbm)[kind]
        target = (wk, wv, wq, wo)[kind]
        return pltpu.make_async_copy(
            source.at[layer], target.at[layer], w_sem.at[kind, layer]
        )

    x_copy = pltpu.make_async_copy(tokens, x0, x_sem)
    small = [
        pltpu.make_async_copy(source, target, small_sem.at[index])
        for index, (source, target) in enumerate(
            ((table_hbm, table), (gain_hbm, gain), (shift_hbm, shift))
        )
    ]

    def halo_copy(kind, layer, seg):
        buffer = (kx, vx)[kind]
        return pltpu.make_async_remote_copy(
            src_ref=buffer.at[layer, pl.ds(reach + seg * SEG, SEG)],
            dst_ref=buffer.at[layer, pl.ds(seg * SEG, SEG)],
            send_sem=halo_send.at[kind, layer, seg],
            recv_sem=halo_recv.at[kind, layer, seg],
            device_id=(jnp.minimum(sp + 1, sp_count - 1), tp),
            device_id_type=MESH,
        )

    def pair_copy(layer, piece):
        first, last = piece
        block = att.at[layer, tp, pl.ds(first * SEG, (last - first) * SEG)]
        return pltpu.make_async_remote_copy(
            src_ref=block,
            dst_ref=block,
            send_sem=pair_send.at[layer, first],
            recv_sem=pair_recv.at[layer, first],
            device_id=(sp, 1 - tp),
            device_id_type=MESH,
        )

    x_copy.start()
    w_copy(0, 0).start()
    w_copy(1, 0).start()

    barrier = pltpu.get_barrier_semaphore()
    pl.semaphore_signal(barrier, inc=1, device_id=(sp, 1 - tp), device_id_type=MESH)

    @pl.when(has_next)
    def _():
        pl.semaphore_signal(barrier, inc=1, device_id=(sp + 1, tp), device_id_type=MESH)

    @pl.when(has_prev)
    def _():
        pl.semaphore_signal(barrier, inc=1, device_id=(sp - 1, tp), device_id_type=MESH)

    @pl.when(jnp.logical_not(has_prev))
    def _():
        for layer in range(LAYERS):
            kx[layer, :reach, :] = jnp.zeros((reach, width), jnp.bfloat16)
            vx[layer, :reach, :] = jnp.zeros((reach, width), jnp.bfloat16)

    lane = lax.broadcasted_iota(jnp.int32, (1, width), 1)
    in_head = [
        (lane >= h * head_size) & (lane < (h + 1) * head_size) for h in range(heads)
    ]

    def build_bias():
        wide = bias.shape[2]
        size = padded.shape[1]
        padded[...] = jnp.zeros_like(padded)
        for layer in range(LAYERS):
            padded[layer * heads : (layer + 1) * heads, : table.shape[2]] = table[layer]
        place = lax.broadcasted_iota(jnp.int32, (size, wide), 1)
        source = lax.broadcasted_iota(jnp.int32, (size, wide), 0)
        onehot = (jnp.clip(band - 1 - place, -CLIP, CLIP) + CLIP == source).astype(jnp.float32)
        by_offset = jnp.dot(
            padded[...],
            onehot,
            precision=lax.Precision.HIGHEST,
            preferred_element_type=jnp.float32,
        )
        for layer in range(LAYERS):
            for h in range(heads):
                line = by_offset[layer * heads + h : layer * heads + h + 1, :]
                skewed = pltpu.roll(
                    jnp.broadcast_to(line, (SEG, wide)), wide - SEG + 1, 1, stride=1, stride_axis=0
                )
                bias[layer, h * SEG : (h + 1) * SEG, :] = skewed

    def project(hidden, layer, piece, kind):
        part = slice(piece[0] * SEG, piece[1] * SEG)
        weight = (wk, wv, wq)[kind]
        return jnp.dot(
            hidden[part, :], weight[layer], preferred_element_type=jnp.float32
        ).astype(jnp.bfloat16)

    def keys(hidden, layer, piece):
        part = slice(reach + piece[0] * SEG, reach + piece[1] * SEG)
        kx[layer, part, :] = project(hidden, layer, piece, 0)

        @pl.when(has_next)
        def _():
            halo_copy(0, layer, piece[1] - 1).start()

    def values(hidden, layer, piece):
        part = slice(reach + piece[0] * SEG, reach + piece[1] * SEG)
        vx[layer, part, :] = project(hidden, layer, piece, 1)

        @pl.when(has_next)
        def _():
            halo_copy(1, layer, piece[1] - 1).start()
            for seg in range(piece[0], piece[1] - 1)[::-1]:
                halo_copy(0, layer, seg).start()
                halo_copy(1, layer, seg).start()

    def queries(hidden, layer, piece):
        part = slice(piece[0] * SEG, piece[1] * SEG)
        query[layer, part, :] = project(hidden, layer, piece, 2) * jnp.bfloat16(head_size**-0.5)

    def attend(layer, seg):
        @pl.when(has_prev)
        def _():
            halo_copy(0, layer, seg).wait_recv()
            halo_copy(1, layer, seg).wait_recv()

        column = lax.broadcasted_iota(jnp.int32, (1, band), 1)
        block = query[layer, seg * SEG : (seg + 1) * SEG, :]
        stacked = jnp.concatenate(
            [jnp.where(in_head[h], block, jnp.zeros_like(block)) for h in range(heads)], axis=0
        )
        key_band = kx[layer, seg * SEG : seg * SEG + band, :]
        value_band = vx[layer, seg * SEG : seg * SEG + band, :]
        scores = lax.dot_general(
            stacked, key_band, (((1,), (1,)), ((), ())), preferred_element_type=jnp.float32
        )
        outside = (column < reach - seg * SEG) & jnp.logical_not(has_prev)
        scores = jnp.where(outside, masked_score, scores + bias[layer, :, :band])
        peak = jnp.max(scores, -1, keepdims=True)
        expo = jnp.exp(scores - peak)
        norm = jnp.sum(expo, -1, keepdims=True)
        mixed = jnp.dot(
            expo.astype(jnp.bfloat16), value_band, preferred_element_type=jnp.float32
        )
        mixed = mixed * (1.0 / norm)
        own = mixed[:SEG, :]
        for h in range(1, heads):
            own = jnp.where(in_head[h], mixed[h * SEG : (h + 1) * SEG, :], own)
        att[layer, tp, seg * SEG : (seg + 1) * SEG, :] = own.astype(jnp.bfloat16)

    def finish(hidden, layer, piece):
        part = slice(piece[0] * SEG, piece[1] * SEG)
        count = (piece[1] - piece[0]) * SEG

        def half(owner):
            weight = wo[layer, pl.ds(pl.multiple_of(owner * width, width), width), :]
            return jnp.dot(att[layer, owner, part, :], weight, preferred_element_type=jnp.float32)

        total[:count, :] = half(tp) + residual_scale * hidden[part, :].astype(jnp.float32)
        pair_copy(layer, piece).wait_recv()
        total[:count, :] += half(1 - tp)
        step = 16
        for r in range(0, count, step):
            here = slice(piece[0] * SEG + r, piece[0] * SEG + r + step)
            value = total[r : r + step, :]
            mean = jnp.sum(value, -1, keepdims=True) * (1.0 / model)
            centred = value - mean
            variance = jnp.sum(centred * centred, -1, keepdims=True) * (1.0 / model)
            scale = lax.rsqrt(variance + norm_eps)
            if layer < LAYERS - 1:
                x1[here, :] = (
                    centred * scale * gain[layer : layer + 1, :] + shift[layer : layer + 1, :]
                ).astype(jnp.bfloat16)
            else:
                cols = pl.ds(pl.multiple_of(tp * (model // 2), model // 2), model // 2)
                out[here, :] = (
                    (total[r : r + step, cols] - mean) * scale * gain[layer : layer + 1, cols]
                    + shift[layer : layer + 1, cols]
                ).astype(jnp.bfloat16)

    every = (0, segments)
    x_copy.wait()
    w_copy(0, 0).wait()
    for copy in (w_copy(2, 0), w_copy(3, 0), *small):
        copy.start()
    pl.semaphore_wait(barrier, 1 + has_next.astype(jnp.int32) + has_prev.astype(jnp.int32))
    keys(x0, 0, every)
    w_copy(1, 0).wait()
    values(x0, 0, every)
    w_copy(2, 0).wait()
    queries(x0, 0, every)
    for kind in range(4):
        w_copy(kind, 1).start()
    for copy in small:
        copy.wait()
    build_bias()
    w_copy(3, 0).wait()

    for seg in range(*late)[::-1]:
        attend(0, seg)
    pair_copy(0, late).start()
    for seg in range(early[0] + 1, early[1])[::-1]:
        attend(0, seg)
    finish(x0, 0, late)
    w_copy(0, 1).wait()
    w_copy(1, 1).wait()
    keys(x1, 1, late)
    values(x1, 1, late)
    attend(0, 0)
    pair_copy(0, early).start()
    w_copy(2, 1).wait()
    w_copy(3, 1).wait()
    queries(x1, 1, late)
    finish(x0, 0, early)
    keys(x1, 1, early)
    values(x1, 1, early)
    queries(x1, 1, early)

    for seg in range(*late)[::-1]:
        attend(1, seg)
    pair_copy(1, late).start()
    pieces = [(seg, seg + 1) for seg in range(*early)[::-1]]
    waiting = late
    for piece in pieces:
        attend(1, piece[0])
        pair_copy(1, piece).start()
        finish(x1, 1, waiting)
        waiting = piece
    finish(x1, 1, waiting)

    for layer, piece in [(0, late), (0, early), (1, late)] + [(1, piece) for piece in pieces]:
        pair_copy(layer, piece).wait_send()

    @pl.when(has_next)
    def _():
        for layer in range(LAYERS):
            for seg in range(segments):
                for kind in range(2):
                    halo_copy(kind, layer, seg).wait_send()


def body(
    sp_count, tokens, query_weight, key_weight, value_weight, out_weight, rel_table, norm_gain,
    norm_bias,
):
    rows, model = tokens.shape
    width = query_weight.shape[2]
    heads = rel_table.shape[1]
    reach = LEFT * SEG
    segments = rows // SEG
    wide = -(-(reach + 2 * SEG - 1) // LANES) * LANES
    size = -(-rel_table.shape[2] // LANES) * LANES
    hbm = pl.BlockSpec(memory_space=pltpu.MemorySpace.HBM)
    vmem = pl.BlockSpec(memory_space=pltpu.VMEM)
    bf16 = jnp.bfloat16
    return pl.pallas_call(
        functools.partial(kernel, sp_count, heads),
        out_shape=jax.ShapeDtypeStruct((rows, model // 2), bf16),
        in_specs=[hbm] * 8,
        out_specs=vmem,
        scratch_shapes=[
            pltpu.VMEM((rows, model), bf16),
            pltpu.VMEM((rows, model), bf16),
            pltpu.VMEM(query_weight.shape, bf16),
            pltpu.VMEM(key_weight.shape, bf16),
            pltpu.VMEM(value_weight.shape, bf16),
            pltpu.VMEM(out_weight.shape, bf16),
            pltpu.VMEM(rel_table.shape, jnp.float32),
            pltpu.VMEM(norm_gain.shape, jnp.float32),
            pltpu.VMEM(norm_bias.shape, jnp.float32),
            pltpu.VMEM((LAYERS, rows, width), bf16),
            pltpu.VMEM((LAYERS, reach + rows, width), bf16),
            pltpu.VMEM((LAYERS, reach + rows, width), bf16),
            pltpu.VMEM((LAYERS, 2, rows, width), bf16),
            pltpu.VMEM((rows // 2, model), jnp.float32),
            pltpu.VMEM((LAYERS, heads * SEG, wide), jnp.float32),
            pltpu.VMEM((-(-LAYERS * heads // 8) * 8, size), jnp.float32),
            pltpu.SemaphoreType.DMA,
            pltpu.SemaphoreType.DMA((4, LAYERS)),
            pltpu.SemaphoreType.DMA((3,)),
            pltpu.SemaphoreType.DMA((2, LAYERS, segments)),
            pltpu.SemaphoreType.DMA((2, LAYERS, segments)),
            pltpu.SemaphoreType.DMA((LAYERS, segments)),
            pltpu.SemaphoreType.DMA((LAYERS, segments)),
        ],
        compiler_params=pltpu.CompilerParams(
            collective_id=0, has_side_effects=True, vmem_limit_bytes=56000000
        ),
    )(
        *(
            pltpu.with_memory_space_constraint(operand, pltpu.MemorySpace.HBM)
            for operand in (
                tokens,
                query_weight,
                key_weight,
                value_weight,
                out_weight,
                rel_table,
                norm_gain,
                norm_bias,
            )
        )
    )


def solution(mesh):
    return jax.shard_map(
        functools.partial(body, mesh.shape["sp"]),
        mesh=mesh,
        in_specs=(
            P("sp", None),
            P(None, None, "tp"),
            P(None, None, "tp"),
            P(None, None, "tp"),
            P(),
            P(None, "tp", None),
            P(),
            P(),
        ),
        out_specs=P("sp", "tp"),
        check_vma=False,
    )
```

profile of v0, /device:TPU:25, one launch (start us, length us, event | category | flops | bytes accessed | tf_op | source)
XLA Modules:
  0.0 23.5 jit_solution(11361761935228691951)
XLA Ops:
  0.0 22.7 %shard_map.82 = bf16[256,1024]{1,0:T(8,128)(2,1)S(1)} custom-call(bf16[256,2048]{1,0:T(8,128)(2,1)} %tokens.1, bf16[2,2048,256]{2,1,0:T(8,128)(2,1)} %wq_hbm.1, bf16[2,2048,256]{2,1,0:T(8,128)(2,1)} %wk_hbm.1, bf16[2,2048,256]{2,1,0:T(8,128)(2,1)} %wv_hbm.1, bf16[2,512,2048]{2,1,0:T(8,128)(2,1)} %wo_hbm.1, f32[2,4,257]{2,1,0:T(4,128)} %table_hbm.1, ...), custom_call_target="tpu_custom_call" | custom-call | tf_op jit(solution)/shard_map/pallas_call | solution.py:323
  22.7 0.8 %copy.10 = bf16[256,1024]{1,0:T(8,128)(2,1)} copy(bf16[256,1024]{1,0:T(8,128)(2,1)S(1)} %shard_map.82) | data formatting | bytes 1048576
where the time goes:
time: 23.6 us; the launch traced here: 23.5 us
  Pallas kernels  22.7 us (96%)
  local copies, waits for them, and re-layouts  0.8 us (3%)
    pallas_call x1, Pallas kernels, body(): pl.pallas_call(functools.partial(kernel, sp_count, heads), out_shape=jax....  22.7 us
    unnamed x1, local copies, waits for them, and re-layouts  0.8 us

commit v1 on v0

--- a/solution.py
+++ b/solution.py
@@ -65,8 +65,6 @@
     tp = lax.axis_index("tp")
     has_next = sp < sp_count - 1
     has_prev = sp > 0
-    late = (segments // 2, segments)
-    early = (0, segments // 2)
 
     def w_copy(kind, layer):
         source = (wk_hbm, wv_hbm, wq_hbm, wo_hbm)[kind]
@@ -75,7 +73,12 @@
             source.at[layer], target.at[layer], w_sem.at[kind, layer]
         )
 
-    x_copy = pltpu.make_async_copy(tokens, x0, x_sem)
+    def x_copy(index, first, count):
+        part = pl.ds(first, count)
+        return pltpu.make_async_copy(tokens.at[part], x0.at[part], x_sem.at[index])
+
+    x_last = x_copy(0, rows - SEG, SEG)
+    x_rest = x_copy(1, 0, rows - SEG)
     small = [
         pltpu.make_async_copy(source, target, small_sem.at[index])
         for index, (source, target) in enumerate(
@@ -94,21 +97,22 @@
             device_id_type=MESH,
         )
 
-    def pair_copy(layer, piece):
-        first, last = piece
-        block = att.at[layer, tp, pl.ds(first * SEG, (last - first) * SEG)]
+    def pair_copy(layer, seg):
+        block = att.at[layer, tp, pl.ds(seg * SEG, SEG)]
         return pltpu.make_async_remote_copy(
             src_ref=block,
             dst_ref=block,
-            send_sem=pair_send.at[layer, first],
-            recv_sem=pair_recv.at[layer, first],
+            send_sem=pair_send.at[layer, seg],
+            recv_sem=pair_recv.at[layer, seg],
             device_id=(sp, 1 - tp),
             device_id_type=MESH,
         )
 
-    x_copy.start()
+    x_last.start()
     w_copy(0, 0).start()
     w_copy(1, 0).start()
+    x_rest.start()
+    w_copy(2, 0).start()
 
     barrier = pltpu.get_barrier_semaphore()
     pl.semaphore_signal(barrier, inc=1, device_id=(sp, 1 - tp), device_id_type=MESH)
@@ -155,42 +159,42 @@
                 )
                 bias[layer, h * SEG : (h + 1) * SEG, :] = skewed
 
-    def project(hidden, layer, piece, kind):
-        part = slice(piece[0] * SEG, piece[1] * SEG)
+    def rows_of(piece):
+        return slice(piece[0] * SEG, piece[1] * SEG)
+
+    def project(hidden, layer, part, kind):
         weight = (wk, wv, wq)[kind]
         return jnp.dot(
             hidden[part, :], weight[layer], preferred_element_type=jnp.float32
         ).astype(jnp.bfloat16)
 
-    def keys(hidden, layer, piece):
-        part = slice(reach + piece[0] * SEG, reach + piece[1] * SEG)
-        kx[layer, part, :] = project(hidden, layer, piece, 0)
+    def keys_values(hidden, layer, piece):
+        part = rows_of(piece)
+        target = slice(reach + part.start, reach + part.stop)
+        kx[layer, target, :] = project(hidden, layer, part, 0)
+        vx[layer, target, :] = project(hidden, layer, part, 1)
 
         @pl.when(has_next)
         def _():
-            halo_copy(0, layer, piece[1] - 1).start()
-
-    def values(hidden, layer, piece):
-        part = slice(reach + piece[0] * SEG, reach + piece[1] * SEG)
-        vx[layer, part, :] = project(hidden, layer, piece, 1)
-
-        @pl.when(has_next)
-        def _():
-            halo_copy(1, layer, piece[1] - 1).start()
-            for seg in range(piece[0], piece[1] - 1)[::-1]:
+            for seg in range(*piece)[::-1]:
                 halo_copy(0, layer, seg).start()
                 halo_copy(1, layer, seg).start()
 
     def queries(hidden, layer, piece):
-        part = slice(piece[0] * SEG, piece[1] * SEG)
-        query[layer, part, :] = project(hidden, layer, piece, 2) * jnp.bfloat16(head_size**-0.5)
-
-    def attend(layer, seg):
+        first, last = piece[0] * SEG, piece[1] * SEG
+        middle = (first + last) // 2
+        for part in (slice(first, middle), slice(middle, last)):
+            query[layer, part, :] = project(hidden, layer, part, 2) * jnp.bfloat16(
+                head_size**-0.5
+            )
+
+    def wait_halo(layer, seg):
         @pl.when(has_prev)
         def _():
             halo_copy(0, layer, seg).wait_recv()
             halo_copy(1, layer, seg).wait_recv()
 
+    def attend(layer, seg):
         column = lax.broadcasted_iota(jnp.int32, (1, band), 1)
         block = query[layer, seg * SEG : (seg + 1) * SEG, :]
         stacked = jnp.concatenate(
@@ -215,21 +219,26 @@
             own = jnp.where(in_head[h], mixed[h * SEG : (h + 1) * SEG, :], own)
         att[layer, tp, seg * SEG : (seg + 1) * SEG, :] = own.astype(jnp.bfloat16)
 
-    def finish(hidden, layer, piece):
-        part = slice(piece[0] * SEG, piece[1] * SEG)
-        count = (piece[1] - piece[0]) * SEG
-
-        def half(owner):
-            weight = wo[layer, pl.ds(pl.multiple_of(owner * width, width), width), :]
-            return jnp.dot(att[layer, owner, part, :], weight, preferred_element_type=jnp.float32)
-
-        total[:count, :] = half(tp) + residual_scale * hidden[part, :].astype(jnp.float32)
-        pair_copy(layer, piece).wait_recv()
-        total[:count, :] += half(1 - tp)
+    def half(layer, owner, seg):
+        weight = wo[layer, pl.ds(pl.multiple_of(owner * width, width), width), :]
+        return jnp.dot(
+            att[layer, owner, seg * SEG : (seg + 1) * SEG, :],
+            weight,
+            preferred_element_type=jnp.float32,
+        )
+
+    def own_half(hidden, layer, seg):
+        part = slice(seg * SEG, (seg + 1) * SEG)
+        total[seg % 2] = half(layer, tp, seg) + residual_scale * hidden[part, :].astype(
+            jnp.float32
+        )
+
+    def finish(layer, seg):
+        total[seg % 2] += half(layer, 1 - tp, seg)
         step = 16
-        for r in range(0, count, step):
-            here = slice(piece[0] * SEG + r, piece[0] * SEG + r + step)
-            value = total[r : r + step, :]
+        for r in range(0, SEG, step):
+            here = slice(seg * SEG + r, seg * SEG + r + step)
+            value = total[seg % 2, r : r + step, :]
             mean = jnp.sum(value, -1, keepdims=True) * (1.0 / model)
             centred = value - mean
             variance = jnp.sum(centred * centred, -1, keepdims=True) * (1.0 / model)
@@ -241,62 +250,78 @@
             else:
                 cols = pl.ds(pl.multiple_of(tp * (model // 2), model // 2), model // 2)
                 out[here, :] = (
-                    (total[r : r + step, cols] - mean) * scale * gain[layer : layer + 1, cols]
+                    (total[seg % 2, r : r + step, cols] - mean)
+                    * scale
+                    * gain[layer : layer + 1, cols]
                     + shift[layer : layer + 1, cols]
                 ).astype(jnp.bfloat16)
 
-    every = (0, segments)
-    x_copy.wait()
+    last = segments - 1
+    scope = jax.named_scope
+    x_last.wait()
     w_copy(0, 0).wait()
-    for copy in (w_copy(2, 0), w_copy(3, 0), *small):
+    w_copy(1, 0).wait()
+    with scope("barrier"):
+        pl.semaphore_wait(barrier, 1 + has_next.astype(jnp.int32) + has_prev.astype(jnp.int32))
+    with scope("kv_last"):
+        keys_values(x0, 0, (last, segments))
+    with scope("x_rest"):
+        x_rest.wait()
+    for copy in (w_copy(3, 0), *small):
         copy.start()
-    pl.semaphore_wait(barrier, 1 + has_next.astype(jnp.int32) + has_prev.astype(jnp.int32))
-    keys(x0, 0, every)
-    w_copy(1, 0).wait()
-    values(x0, 0, every)
+    with scope("kv_rest"):
+        keys_values(x0, 0, (0, last))
     w_copy(2, 0).wait()
-    queries(x0, 0, every)
+    with scope("queries"):
+        queries(x0, 0, (0, segments))
     for kind in range(4):
         w_copy(kind, 1).start()
     for copy in small:
         copy.wait()
-    build_bias()
+    with scope("bias"):
+        build_bias()
     w_copy(3, 0).wait()
 
-    for seg in range(*late)[::-1]:
-        attend(0, seg)
-    pair_copy(0, late).start()
-    for seg in range(early[0] + 1, early[1])[::-1]:
-        attend(0, seg)
-    finish(x0, 0, late)
-    w_copy(0, 1).wait()
-    w_copy(1, 1).wait()
-    keys(x1, 1, late)
-    values(x1, 1, late)
-    attend(0, 0)
-    pair_copy(0, early).start()
-    w_copy(2, 1).wait()
-    w_copy(3, 1).wait()
-    queries(x1, 1, late)
-    finish(x0, 0, early)
-    keys(x1, 1, early)
-    values(x1, 1, early)
-    queries(x1, 1, early)
-
-    for seg in range(*late)[::-1]:
-        attend(1, seg)
-    pair_copy(1, late).start()
-    pieces = [(seg, seg + 1) for seg in range(*early)[::-1]]
-    waiting = late
-    for piece in pieces:
-        attend(1, piece[0])
-        pair_copy(1, piece).start()
-        finish(x1, 1, waiting)
-        waiting = piece
-    finish(x1, 1, waiting)
-
-    for layer, piece in [(0, late), (0, early), (1, late)] + [(1, piece) for piece in pieces]:
-        pair_copy(layer, piece).wait_send()
+    hiddens = (x0, x1)
+    for layer in range(LAYERS):
+        waiting = None
+        for seg in range(segments)[::-1]:
+            with scope(f"halo_{layer}_{seg}"):
+                wait_halo(layer, seg)
+            with scope(f"attend_{layer}_{seg}"):
+                attend(layer, seg)
+                pair_copy(layer, seg).start()
+                if waiting is not None:
+                    own_half(hiddens[layer], layer, waiting)
+            if waiting is not None:
+                with scope(f"pair_{layer}_{waiting}"):
+                    pair_copy(layer, waiting).wait_recv()
+                with scope(f"finish_{layer}_{waiting}"):
+                    finish(layer, waiting)
+                if layer < LAYERS - 1:
+                    if waiting == last:
+                        w_copy(0, layer + 1).wait()
+                        w_copy(1, layer + 1).wait()
+                    with scope(f"kv_{layer}_{waiting}"):
+                        keys_values(hiddens[layer + 1], layer + 1, (waiting, waiting + 1))
+            waiting = seg
+        with scope(f"own_{layer}"):
+            own_half(hiddens[layer], layer, waiting)
+        with scope(f"pair_{layer}_{waiting}"):
+            pair_copy(layer, waiting).wait_recv()
+        with scope(f"finish_{layer}_{waiting}"):
+            finish(layer, waiting)
+        if layer < LAYERS - 1:
+            with scope(f"kv_{layer}_{waiting}"):
+                keys_values(hiddens[layer + 1], layer + 1, (waiting, waiting + 1))
+            w_copy(2, layer + 1).wait()
+            w_copy(3, layer + 1).wait()
+            with scope(f"queries_{layer}"):
+                queries(hiddens[layer + 1], layer + 1, (0, segments))
+
+    for layer in range(LAYERS):
+        for seg in range(segments):
+            pair_copy(layer, seg).wait_send()
 
     @pl.when(has_next)
     def _():
@@ -339,10 +364,10 @@
             pltpu.VMEM((LAYERS, reach + rows, width), bf16),
             pltpu.VMEM((LAYERS, reach + rows, width), bf16),
             pltpu.VMEM((LAYERS, 2, rows, width), bf16),
-            pltpu.VMEM((rows // 2, model), jnp.float32),
+            pltpu.VMEM((2, SEG, model), jnp.float32),
             pltpu.VMEM((LAYERS, heads * SEG, wide), jnp.float32),
             pltpu.VMEM((-(-LAYERS * heads // 8) * 8, size), jnp.float32),
-            pltpu.SemaphoreType.DMA,
+            pltpu.SemaphoreType.DMA((2,)),
             pltpu.SemaphoreType.DMA((4, LAYERS)),
             pltpu.SemaphoreType.DMA((3,)),
             pltpu.SemaphoreType.DMA((2, LAYERS, segments)),

time: 23.6 us -> 23.7 us (level)
  no operation moved by 1% of the time
where the time goes in v1:
time: 23.7 us; the launch traced here: 23.6 us
  Pallas kernels  22.8 us (96%)
  local copies, waits for them, and re-layouts  0.8 us (3%)
    pallas_call x1, Pallas kernels, body(): pl.pallas_call(functools.partial(kernel, sp_count, heads), out_shape=jax....  22.8 us
    unnamed x1, local copies, waits for them, and re-layouts  0.8 us

profile of v1, /device:TPU:25, one launch (start us, length us, event | category | flops | bytes accessed | tf_op | source)
XLA Modules:
  0.0 23.6 jit_solution(1204110911707315112)
XLA Ops:
  0.0 22.8 %shard_map.82 = bf16[256,1024]{1,0:T(8,128)(2,1)S(1)} custom-call(bf16[256,2048]{1,0:T(8,128)(2,1)} %tokens.1, bf16[2,2048,256]{2,1,0:T(8,128)(2,1)} %wq_hbm.1, bf16[2,2048,256]{2,1,0:T(8,128)(2,1)} %wk_hbm.1, bf16[2,2048,256]{2,1,0:T(8,128)(2,1)} %wv_hbm.1, bf16[2,512,2048]{2,1,0:T(8,128)(2,1)} %wo_hbm.1, f32[2,4,257]{2,1,0:T(4,128)} %table_hbm.1, ...), custom_call_target="tpu_custom_call" | custom-call | tf_op jit(solution)/shard_map/pallas_call | solution.py:348
  22.8 0.8 %copy.10 = bf16[256,1024]{1,0:T(8,128)(2,1)} copy(bf16[256,1024]{1,0:T(8,128)(2,1)S(1)} %shard_map.82) | data formatting | bytes 1048576

commit v2 on v1

--- a/solution.py
+++ b/solution.py
@@ -12,6 +12,7 @@
 CLIP = 128
 LAYERS = 2
 LANES = 128
+CHUNKS = 4
 
 residual_scale = 2.0**0.5
 norm_eps = 1e-05
@@ -44,10 +45,12 @@
     kx,
     vx,
     att,
+    peer,
     total,
     bias,
     padded,
     x_sem,
+    first_sem,
     w_sem,
     small_sem,
     halo_send,
@@ -66,12 +69,25 @@
     has_next = sp < sp_count - 1
     has_prev = sp > 0
 
+    def first_copy(kind, index):
+        size = model // CHUNKS
+        part = pl.ds(index * size, size)
+        return pltpu.make_async_copy(
+            (wk_hbm, wv_hbm)[kind].at[0, part],
+            (wk, wv)[kind].at[0, part],
+            first_sem.at[kind, index],
+        )
+
     def w_copy(kind, layer):
-        source = (wk_hbm, wv_hbm, wq_hbm, wo_hbm)[kind]
-        target = (wk, wv, wq, wo)[kind]
-        return pltpu.make_async_copy(
-            source.at[layer], target.at[layer], w_sem.at[kind, layer]
-        )
+        if kind < 3:
+            source = (wk_hbm, wv_hbm, wq_hbm)[kind].at[layer]
+            target = (wk, wv, wq)[kind].at[layer]
+        else:
+            owner = (tp, 1 - tp)[kind - 3]
+            part = pl.ds(pl.multiple_of(owner * width, width), width)
+            source = wo_hbm.at[layer, part]
+            target = wo.at[layer, kind - 3]
+        return pltpu.make_async_copy(source, target, w_sem.at[kind, layer])
 
     def x_copy(index, first, count):
         part = pl.ds(first, count)
@@ -98,10 +114,10 @@
         )
 
     def pair_copy(layer, seg):
-        block = att.at[layer, tp, pl.ds(seg * SEG, SEG)]
+        part = pl.ds(seg * SEG, SEG)
         return pltpu.make_async_remote_copy(
-            src_ref=block,
-            dst_ref=block,
+            src_ref=att.at[layer, part],
+            dst_ref=peer.at[layer, part],
             send_sem=pair_send.at[layer, seg],
             recv_sem=pair_recv.at[layer, seg],
             device_id=(sp, 1 - tp),
@@ -109,17 +125,14 @@
         )
 
     x_last.start()
-    w_copy(0, 0).start()
-    w_copy(1, 0).start()
+    first = [first_copy(kind, index) for kind in range(2) for index in range(CHUNKS)]
+    for copy in first:
+        copy.start()
     x_rest.start()
     w_copy(2, 0).start()
 
     barrier = pltpu.get_barrier_semaphore()
     pl.semaphore_signal(barrier, inc=1, device_id=(sp, 1 - tp), device_id_type=MESH)
-
-    @pl.when(has_next)
-    def _():
-        pl.semaphore_signal(barrier, inc=1, device_id=(sp + 1, tp), device_id_type=MESH)
 
     @pl.when(has_prev)
     def _():
@@ -130,11 +143,6 @@
         for layer in range(LAYERS):
             kx[layer, :reach, :] = jnp.zeros((reach, width), jnp.bfloat16)
             vx[layer, :reach, :] = jnp.zeros((reach, width), jnp.bfloat16)
-
-    lane = lax.broadcasted_iota(jnp.int32, (1, width), 1)
-    in_head = [
-        (lane >= h * head_size) & (lane < (h + 1) * head_size) for h in range(heads)
-    ]
 
     def build_bias():
         wide = bias.shape[2]
@@ -180,61 +188,115 @@
                 halo_copy(0, layer, seg).start()
                 halo_copy(1, layer, seg).start()
 
+    def project_split(hidden, layer, part, kind):
+        weight = (wk, wv, wq)[kind]
+        return [
+            jnp.dot(
+                hidden[part, :],
+                weight[layer, :, first : first + LANES],
+                preferred_element_type=jnp.float32,
+            ).astype(jnp.bfloat16)
+            for first in range(0, width, LANES)
+        ]
+
+    def keys(hidden, layer, seg):
+        target = slice(reach + seg * SEG, reach + (seg + 1) * SEG)
+        for group, block in enumerate(
+            project_split(hidden, layer, slice(seg * SEG, (seg + 1) * SEG), 0)
+        ):
+            kx[layer, target, group * LANES : (group + 1) * LANES] = block
+
+        @pl.when(has_next)
+        def _():
+            halo_copy(0, layer, seg).start()
+
+    def values(hidden, layer, seg):
+        target = slice(reach + seg * SEG, reach + (seg + 1) * SEG)
+        for group, block in enumerate(
+            project_split(hidden, layer, slice(seg * SEG, (seg + 1) * SEG), 1)
+        ):
+            vx[layer, target, group * LANES : (group + 1) * LANES] = block
+
+        @pl.when(has_next)
+        def _():
+            halo_copy(1, layer, seg).start()
+
     def queries(hidden, layer, piece):
         first, last = piece[0] * SEG, piece[1] * SEG
-        middle = (first + last) // 2
+        middle = (first + last) // 2 if last - first > SEG else last
         for part in (slice(first, middle), slice(middle, last)):
+            if part.start == part.stop:
+                continue
             query[layer, part, :] = project(hidden, layer, part, 2) * jnp.bfloat16(
                 head_size**-0.5
             )
 
-    def wait_halo(layer, seg):
+    def wait_halo(layer, seg, kind=None):
         @pl.when(has_prev)
         def _():
-            halo_copy(0, layer, seg).wait_recv()
-            halo_copy(1, layer, seg).wait_recv()
-
-    def attend(layer, seg):
+            for each in (0, 1) if kind is None else (kind,):
+                halo_copy(each, layer, seg).wait_recv()
+
+    pair = LANES // head_size
+    lane = lax.broadcasted_iota(jnp.int32, (1, LANES), 1)
+    in_pair = [
+        (lane >= h * head_size) & (lane < (h + 1) * head_size) for h in range(pair)
+    ]
+
+    def scores(layer, seg):
         column = lax.broadcasted_iota(jnp.int32, (1, band), 1)
-        block = query[layer, seg * SEG : (seg + 1) * SEG, :]
-        stacked = jnp.concatenate(
-            [jnp.where(in_head[h], block, jnp.zeros_like(block)) for h in range(heads)], axis=0
-        )
-        key_band = kx[layer, seg * SEG : seg * SEG + band, :]
-        value_band = vx[layer, seg * SEG : seg * SEG + band, :]
-        scores = lax.dot_general(
-            stacked, key_band, (((1,), (1,)), ((), ())), preferred_element_type=jnp.float32
-        )
         outside = (column < reach - seg * SEG) & jnp.logical_not(has_prev)
-        scores = jnp.where(outside, masked_score, scores + bias[layer, :, :band])
-        peak = jnp.max(scores, -1, keepdims=True)
-        expo = jnp.exp(scores - peak)
-        norm = jnp.sum(expo, -1, keepdims=True)
-        mixed = jnp.dot(
-            expo.astype(jnp.bfloat16), value_band, preferred_element_type=jnp.float32
-        )
-        mixed = mixed * (1.0 / norm)
-        own = mixed[:SEG, :]
-        for h in range(1, heads):
-            own = jnp.where(in_head[h], mixed[h * SEG : (h + 1) * SEG, :], own)
-        att[layer, tp, seg * SEG : (seg + 1) * SEG, :] = own.astype(jnp.bfloat16)
-
-    def half(layer, owner, seg):
-        weight = wo[layer, pl.ds(pl.multiple_of(owner * width, width), width), :]
+        results = []
+        for group in range(width // LANES):
+            lanes = slice(group * LANES, (group + 1) * LANES)
+            block = query[layer, seg * SEG : (seg + 1) * SEG, lanes]
+            stacked = jnp.concatenate(
+                [jnp.where(in_pair[h], block, jnp.zeros_like(block)) for h in range(pair)], axis=0
+            )
+            raw = lax.dot_general(
+                stacked,
+                kx[layer, seg * SEG : seg * SEG + band, lanes],
+                (((1,), (1,)), ((), ())),
+                preferred_element_type=jnp.float32,
+            )
+            lines = slice(group * pair * SEG, (group + 1) * pair * SEG)
+            results.append(jnp.where(outside, masked_score, raw + bias[layer, lines, :band]))
+        return results
+
+    def weigh(layer, seg, results):
+        for group, raw in enumerate(results):
+            lanes = slice(group * LANES, (group + 1) * LANES)
+            peak = jnp.max(raw, -1, keepdims=True)
+            expo = jnp.exp(raw - peak)
+            norm = jnp.sum(expo, -1, keepdims=True)
+            mixed = jnp.dot(
+                expo.astype(jnp.bfloat16),
+                vx[layer, seg * SEG : seg * SEG + band, lanes],
+                preferred_element_type=jnp.float32,
+            )
+            mixed = mixed * (1.0 / norm)
+            own = mixed[:SEG, :]
+            for h in range(1, pair):
+                own = jnp.where(in_pair[h], mixed[h * SEG : (h + 1) * SEG, :], own)
+            att[layer, seg * SEG : (seg + 1) * SEG, lanes] = own.astype(jnp.bfloat16)
+
+    def half(layer, seg, source, index):
         return jnp.dot(
-            att[layer, owner, seg * SEG : (seg + 1) * SEG, :],
-            weight,
+            source[layer, seg * SEG : (seg + 1) * SEG, :],
+            wo[layer, index],
             preferred_element_type=jnp.float32,
         )
 
     def own_half(hidden, layer, seg):
         part = slice(seg * SEG, (seg + 1) * SEG)
-        total[seg % 2] = half(layer, tp, seg) + residual_scale * hidden[part, :].astype(
+        total[seg % 2] = half(layer, seg, att, 0) + residual_scale * hidden[part, :].astype(
             jnp.float32
         )
 
+    def other_half(layer, seg):
+        total[seg % 2] += half(layer, seg, peer, 1)
+
     def finish(layer, seg):
-        total[seg % 2] += half(layer, 1 - tp, seg)
         step = 16
         for r in range(0, SEG, step):
             here = slice(seg * SEG + r, seg * SEG + r + step)
@@ -258,66 +320,120 @@
 
     last = segments - 1
     scope = jax.named_scope
-    x_last.wait()
-    w_copy(0, 0).wait()
-    w_copy(1, 0).wait()
+    with scope("x_last"):
+        x_last.wait()
+    with scope("w_k"):
+        for copy in first[:CHUNKS]:
+            copy.wait()
     with scope("barrier"):
-        pl.semaphore_wait(barrier, 1 + has_next.astype(jnp.int32) + has_prev.astype(jnp.int32))
-    with scope("kv_last"):
-        keys_values(x0, 0, (last, segments))
+        pl.semaphore_wait(barrier, 1 + has_next.astype(jnp.int32))
+    with scope("k_last"):
+        keys(x0, 0, last)
+    with scope("w_v"):
+        for copy in first[CHUNKS:]:
+            copy.wait()
+    with scope("v_last"):
+        values(x0, 0, last)
     with scope("x_rest"):
         x_rest.wait()
-    for copy in (w_copy(3, 0), *small):
+    for copy in (*small, w_copy(3, 0), w_copy(4, 0)):
         copy.start()
     with scope("kv_rest"):
         keys_values(x0, 0, (0, last))
     w_copy(2, 0).wait()
     with scope("queries"):
         queries(x0, 0, (0, segments))
-    for kind in range(4):
+    for kind in range(5):
         w_copy(kind, 1).start()
     for copy in small:
         copy.wait()
     with scope("bias"):
         build_bias()
     w_copy(3, 0).wait()
+    w_copy(4, 0).wait()
 
     hiddens = (x0, x1)
     for layer in range(LAYERS):
-        waiting = None
-        for seg in range(segments)[::-1]:
-            with scope(f"halo_{layer}_{seg}"):
-                wait_halo(layer, seg)
-            with scope(f"attend_{layer}_{seg}"):
-                attend(layer, seg)
+        hidden = hiddens[layer]
+        more = layer < LAYERS - 1
+        with scope(f"halo_{layer}_{last}"):
+            wait_halo(layer, last)
+        with scope(f"attend_{layer}_{last}"):
+            weigh(layer, last, scores(layer, last))
+        pair_copy(layer, last).start()
+        if more:
+            with scope(f"own_{layer}_{last}"):
+                own_half(hidden, layer, last)
+            for kind in range(5):
+                w_copy(kind, layer + 1).wait()
+            for seg in range(segments)[::-1]:
+                if seg > 0:
+                    with scope(f"halo_{layer}_{seg - 1}"):
+                        wait_halo(layer, seg - 1)
+                with scope(f"pair_{layer}_{seg}"):
+                    pair_copy(layer, seg).wait_recv()
+                with scope(f"block_{layer}_{seg}"):
+                    if seg > 0:
+                        results = scores(layer, seg - 1)
+                    other_half(layer, seg)
+                    if seg > 0:
+                        weigh(layer, seg - 1, results)
+                    finish(layer, seg)
+                if seg > 0:
+                    pair_copy(layer, seg - 1).start()
+                with scope(f"kv_{layer}_{seg}"):
+                    keys_values(hiddens[layer + 1], layer + 1, (seg, seg + 1))
+                with scope(f"own_{layer}_{seg}"):
+                    if seg > 0:
+                        own_half(hidden, layer, seg - 1)
+                    else:
+                        queries(hiddens[layer + 1], layer + 1, (0, segments))
+        else:
+            done = last
+            for seg in range(last)[::-1]:
+                with scope(f"halo_{layer}_{seg}"):
+                    wait_halo(layer, seg, 0)
+                    if seg > 0:
+                        wait_halo(layer, seg, 1)
+                if 0 < seg < last - 1:
+                    with scope(f"pair_{layer}_{done}"):
+                        pair_copy(layer, done).wait_recv()
+                with scope(f"block_{layer}_{seg}"):
+                    results = scores(layer, seg)
+                    if seg == last - 1:
+                        own_half(hidden, layer, last)
+                    elif seg > 0:
+                        other_half(layer, done)
+                    else:
+                        own_half(hidden, layer, seg + 1)
+                    if seg == 0:
+                        with scope("halo_v"):
+                            wait_halo(layer, seg, 1)
+                    weigh(layer, seg, results)
+                    if 0 < seg < last - 1:
+                        finish(layer, done)
                 pair_copy(layer, seg).start()
-                if waiting is not None:
-                    own_half(hiddens[layer], layer, waiting)
-            if waiting is not None:
-                with scope(f"pair_{layer}_{waiting}"):
-                    pair_copy(layer, waiting).wait_recv()
-                with scope(f"finish_{layer}_{waiting}"):
-                    finish(layer, waiting)
-                if layer < LAYERS - 1:
-                    if waiting == last:
-                        w_copy(0, layer + 1).wait()
-                        w_copy(1, layer + 1).wait()
-                    with scope(f"kv_{layer}_{waiting}"):
-                        keys_values(hiddens[layer + 1], layer + 1, (waiting, waiting + 1))
-            waiting = seg
-        with scope(f"own_{layer}"):
-            own_half(hiddens[layer], layer, waiting)
-        with scope(f"pair_{layer}_{waiting}"):
-            pair_copy(layer, waiting).wait_recv()
-        with scope(f"finish_{layer}_{waiting}"):
-            finish(layer, waiting)
-        if layer < LAYERS - 1:
-            with scope(f"kv_{layer}_{waiting}"):
-                keys_values(hiddens[layer + 1], layer + 1, (waiting, waiting + 1))
-            w_copy(2, layer + 1).wait()
-            w_copy(3, layer + 1).wait()
-            with scope(f"queries_{layer}"):
-                queries(hiddens[layer + 1], layer + 1, (0, segments))
+                if 0 < seg < last - 1:
+                    done = done - 1
+                    with scope(f"own_{layer}_{done}"):
+                        own_half(hidden, layer, done)
+                    if seg == 1:
+                        with scope(f"pair_{layer}_{done}"):
+                            pair_copy(layer, done).wait_recv()
+                        with scope(f"finish_{layer}_{done}"):
+                            other_half(layer, done)
+                            finish(layer, done)
+                        done = done - 1
+            while done >= 0:
+                if done == 0:
+                    with scope(f"own_{layer}_{done}"):
+                        own_half(hidden, layer, done)
+                with scope(f"pair_{layer}_{done}"):
+                    pair_copy(layer, done).wait_recv()
+                with scope(f"finish_{layer}_{done}"):
+                    other_half(layer, done)
+                    finish(layer, done)
+                done = done - 1
 
     for layer in range(LAYERS):
         for seg in range(segments):
@@ -356,19 +472,21 @@
             pltpu.VMEM(query_weight.shape, bf16),
             pltpu.VMEM(key_weight.shape, bf16),
             pltpu.VMEM(value_weight.shape, bf16),
-            pltpu.VMEM(out_weight.shape, bf16),
+            pltpu.VMEM((LAYERS, 2, width, model), bf16),
             pltpu.VMEM(rel_table.shape, jnp.float32),
             pltpu.VMEM(norm_gain.shape, jnp.float32),
             pltpu.VMEM(norm_bias.shape, jnp.float32),
             pltpu.VMEM((LAYERS, rows, width), bf16),
             pltpu.VMEM((LAYERS, reach + rows, width), bf16),
             pltpu.VMEM((LAYERS, reach + rows, width), bf16),
-            pltpu.VMEM((LAYERS, 2, rows, width), bf16),
+            pltpu.VMEM((LAYERS, rows, width), bf16),
+            pltpu.VMEM((LAYERS, rows, width), bf16),
             pltpu.VMEM((2, SEG, model), jnp.float32),
             pltpu.VMEM((LAYERS, heads * SEG, wide), jnp.float32),
             pltpu.VMEM((-(-LAYERS * heads // 8) * 8, size), jnp.float32),
             pltpu.SemaphoreType.DMA((2,)),
-            pltpu.SemaphoreType.DMA((4, LAYERS)),
+            pltpu.SemaphoreType.DMA((2, CHUNKS)),
+            pltpu.SemaphoreType.DMA((5, LAYERS)),
             pltpu.SemaphoreType.DMA((3,)),
             pltpu.SemaphoreType.DMA((2, LAYERS, segments)),
             pltpu.SemaphoreType.DMA((2, LAYERS, segments)),

time: 23.7 us -> 21.4 us (0.903)
  Pallas kernels: 22.8 us -> 20.5 us
    pallas_call x1, Pallas kernels: 22.8 us -> 20.5 us  [body(): pl.pallas_call(functools.partial(kernel, sp_count, heads), out_shape=jax....]
where the time goes in v2:
time: 21.4 us; the launch traced here: 21.3 us
  Pallas kernels  20.5 us (96%)
  local copies, waits for them, and re-layouts  0.8 us (4%)
    pallas_call x1, Pallas kernels, body(): pl.pallas_call(functools.partial(kernel, sp_count, heads), out_shape=jax....  20.5 us
    unnamed x1, local copies, waits for them, and re-layouts  0.8 us

profile of v2, /device:TPU:25, one launch (start us, length us, event | category | flops | bytes accessed | tf_op | source)
XLA Modules:
  0.0 21.3 jit_solution(7051585449610049669)
XLA Ops:
  0.0 20.5 %shard_map.82 = bf16[256,1024]{1,0:T(8,128)(2,1)S(1)} custom-call(bf16[256,2048]{1,0:T(8,128)(2,1)} %tokens.1, bf16[2,2048,256]{2,1,0:T(8,128)(2,1)} %wq_hbm.1, bf16[2,2048,256]{2,1,0:T(8,128)(2,1)} %wk_hbm.1, bf16[2,2048,256]{2,1,0:T(8,128)(2,1)} %wv_hbm.1, bf16[2,512,2048]{2,1,0:T(8,128)(2,1)} %wo_hbm.1, f32[2,4,257]{2,1,0:T(4,128)} %table_hbm.1, ...), custom_call_target="tpu_custom_call" | custom-call | tf_op jit(solution)/shard_map/pallas_call | solution.py:464
  20.5 0.8 %copy.10 = bf16[256,1024]{1,0:T(8,128)(2,1)} copy(bf16[256,1024]{1,0:T(8,128)(2,1)S(1)} %shard_map.82) | data formatting | bytes 1048576

commit v3 on v2

--- a/solution.py
+++ b/solution.py
@@ -124,19 +124,22 @@
             device_id_type=MESH,
         )
 
+    barrier = pltpu.get_barrier_semaphore()
+    pl.semaphore_signal(barrier, inc=1, device_id=(sp, 1 - tp), device_id_type=MESH)
+
+    @pl.when(has_prev)
+    def _():
+        pl.semaphore_signal(barrier, inc=1, device_id=(sp - 1, tp), device_id_type=MESH)
+
     x_last.start()
     first = [first_copy(kind, index) for kind in range(2) for index in range(CHUNKS)]
-    for copy in first:
+    for copy in first[:CHUNKS]:
+        copy.start()
+    pl.delay(200)
+    for copy in first[CHUNKS:]:
         copy.start()
     x_rest.start()
     w_copy(2, 0).start()
-
-    barrier = pltpu.get_barrier_semaphore()
-    pl.semaphore_signal(barrier, inc=1, device_id=(sp, 1 - tp), device_id_type=MESH)
-
-    @pl.when(has_prev)
-    def _():
-        pl.semaphore_signal(barrier, inc=1, device_id=(sp - 1, tp), device_id_type=MESH)
 
     @pl.when(jnp.logical_not(has_prev))
     def _():
@@ -199,16 +202,12 @@
             for first in range(0, width, LANES)
         ]
 
-    def keys(hidden, layer, seg):
+    def store_keys(hidden, layer, seg):
         target = slice(reach + seg * SEG, reach + (seg + 1) * SEG)
         for group, block in enumerate(
             project_split(hidden, layer, slice(seg * SEG, (seg + 1) * SEG), 0)
         ):
             kx[layer, target, group * LANES : (group + 1) * LANES] = block
-
-        @pl.when(has_next)
-        def _():
-            halo_copy(0, layer, seg).start()
 
     def values(hidden, layer, seg):
         target = slice(reach + seg * SEG, reach + (seg + 1) * SEG)
@@ -220,6 +219,13 @@
         @pl.when(has_next)
         def _():
             halo_copy(1, layer, seg).start()
+
+    def queries_split(hidden, layer, seg):
+        part = slice(seg * SEG, (seg + 1) * SEG)
+        for group, block in enumerate(project_split(hidden, layer, part, 2)):
+            query[layer, part, group * LANES : (group + 1) * LANES] = block * jnp.bfloat16(
+                head_size**-0.5
+            )
 
     def queries(hidden, layer, piece):
         first, last = piece[0] * SEG, piece[1] * SEG
@@ -263,44 +269,50 @@
             results.append(jnp.where(outside, masked_score, raw + bias[layer, lines, :band]))
         return results
 
-    def weigh(layer, seg, results):
-        for group, raw in enumerate(results):
+    def soften(results):
+        softened = []
+        for raw in results:
+            expo = jnp.exp(raw - jnp.max(raw, -1, keepdims=True))
+            norm = jnp.sum(expo, -1, keepdims=True)
+            softened.append((expo.astype(jnp.bfloat16), 1.0 / norm))
+        return softened
+
+    def weigh(layer, seg, softened):
+        for group, (expo, inverse) in enumerate(softened):
             lanes = slice(group * LANES, (group + 1) * LANES)
-            peak = jnp.max(raw, -1, keepdims=True)
-            expo = jnp.exp(raw - peak)
-            norm = jnp.sum(expo, -1, keepdims=True)
             mixed = jnp.dot(
-                expo.astype(jnp.bfloat16),
+                expo,
                 vx[layer, seg * SEG : seg * SEG + band, lanes],
                 preferred_element_type=jnp.float32,
             )
-            mixed = mixed * (1.0 / norm)
+            mixed = mixed * inverse
             own = mixed[:SEG, :]
             for h in range(1, pair):
                 own = jnp.where(in_pair[h], mixed[h * SEG : (h + 1) * SEG, :], own)
             att[layer, seg * SEG : (seg + 1) * SEG, lanes] = own.astype(jnp.bfloat16)
 
-    def half(layer, seg, source, index):
+    def half(layer, piece, source, index):
         return jnp.dot(
-            source[layer, seg * SEG : (seg + 1) * SEG, :],
+            source[layer, rows_of(piece), :],
             wo[layer, index],
             preferred_element_type=jnp.float32,
         )
 
-    def own_half(hidden, layer, seg):
-        part = slice(seg * SEG, (seg + 1) * SEG)
-        total[seg % 2] = half(layer, seg, att, 0) + residual_scale * hidden[part, :].astype(
+    def own_half(hidden, layer, piece):
+        part = rows_of(piece)
+        total[part, :] = half(layer, piece, att, 0) + residual_scale * hidden[part, :].astype(
             jnp.float32
         )
 
-    def other_half(layer, seg):
-        total[seg % 2] += half(layer, seg, peer, 1)
-
-    def finish(layer, seg):
+    def other_half(layer, piece):
+        total[rows_of(piece), :] += half(layer, piece, peer, 1)
+
+    def finish(layer, piece):
         step = 16
-        for r in range(0, SEG, step):
-            here = slice(seg * SEG + r, seg * SEG + r + step)
-            value = total[seg % 2, r : r + step, :]
+        part = rows_of(piece)
+        for r in range(part.start, part.stop, step):
+            here = slice(r, r + step)
+            value = total[here, :]
             mean = jnp.sum(value, -1, keepdims=True) * (1.0 / model)
             centred = value - mean
             variance = jnp.sum(centred * centred, -1, keepdims=True) * (1.0 / model)
@@ -312,9 +324,7 @@
             else:
                 cols = pl.ds(pl.multiple_of(tp * (model // 2), model // 2), model // 2)
                 out[here, :] = (
-                    (total[seg % 2, r : r + step, cols] - mean)
-                    * scale
-                    * gain[layer : layer + 1, cols]
+                    (total[here, cols] - mean) * scale * gain[layer : layer + 1, cols]
                     + shift[layer : layer + 1, cols]
                 ).astype(jnp.bfloat16)
 
@@ -325,10 +335,15 @@
     with scope("w_k"):
         for copy in first[:CHUNKS]:
             copy.wait()
+    with scope("k_last"):
+        store_keys(x0, 0, last)
     with scope("barrier"):
         pl.semaphore_wait(barrier, 1 + has_next.astype(jnp.int32))
-    with scope("k_last"):
-        keys(x0, 0, last)
+
+    @pl.when(has_next)
+    def _():
+        halo_copy(0, 0, last).start()
+
     with scope("w_v"):
         for copy in first[CHUNKS:]:
             copy.wait()
@@ -352,88 +367,93 @@
     w_copy(3, 0).wait()
     w_copy(4, 0).wait()
 
+    def one(seg):
+        return (seg, seg + 1)
+
     hiddens = (x0, x1)
-    for layer in range(LAYERS):
-        hidden = hiddens[layer]
-        more = layer < LAYERS - 1
-        with scope(f"halo_{layer}_{last}"):
-            wait_halo(layer, last)
-        with scope(f"attend_{layer}_{last}"):
-            weigh(layer, last, scores(layer, last))
+    for layer in range(LAYERS - 1):
+        hidden, following = hiddens[layer], hiddens[layer + 1]
+        with scope(f"k_{layer}_{last}"):
+            wait_halo(layer, last, 0)
+        with scope(f"soften_{layer}_{last}"):
+            softened = soften(scores(layer, last))
+        with scope(f"v_{layer}_{last}"):
+            wait_halo(layer, last, 1)
+        with scope(f"weigh_{layer}_{last}"):
+            weigh(layer, last, softened)
         pair_copy(layer, last).start()
-        if more:
-            with scope(f"own_{layer}_{last}"):
-                own_half(hidden, layer, last)
-            for kind in range(5):
-                w_copy(kind, layer + 1).wait()
-            for seg in range(segments)[::-1]:
+        with scope(f"own_{layer}_{last}"):
+            own_half(hidden, layer, one(last))
+        for kind in range(5):
+            w_copy(kind, layer + 1).wait()
+        for seg in range(segments)[::-1]:
+            if seg > 0:
+                with scope(f"halo_{layer}_{seg - 1}"):
+                    wait_halo(layer, seg - 1)
+            with scope(f"pair_{layer}_{seg}"):
+                pair_copy(layer, seg).wait_recv()
+            with scope(f"block_{layer}_{seg}"):
                 if seg > 0:
-                    with scope(f"halo_{layer}_{seg - 1}"):
-                        wait_halo(layer, seg - 1)
-                with scope(f"pair_{layer}_{seg}"):
-                    pair_copy(layer, seg).wait_recv()
-                with scope(f"block_{layer}_{seg}"):
-                    if seg > 0:
-                        results = scores(layer, seg - 1)
-                    other_half(layer, seg)
-                    if seg > 0:
-                        weigh(layer, seg - 1, results)
-                    finish(layer, seg)
+                    results = scores(layer, seg - 1)
+                other_half(layer, one(seg))
                 if seg > 0:
-                    pair_copy(layer, seg - 1).start()
-                with scope(f"kv_{layer}_{seg}"):
-                    keys_values(hiddens[layer + 1], layer + 1, (seg, seg + 1))
-                with scope(f"own_{layer}_{seg}"):
-                    if seg > 0:
-                        own_half(hidden, layer, seg - 1)
-                    else:
-                        queries(hiddens[layer + 1], layer + 1, (0, segments))
-        else:
-            done = last
-            for seg in range(last)[::-1]:
-                with scope(f"halo_{layer}_{seg}"):
-                    wait_halo(layer, seg, 0)
-                    if seg > 0:
-                        wait_halo(layer, seg, 1)
-                if 0 < seg < last - 1:
-                    with scope(f"pair_{layer}_{done}"):
-                        pair_copy(layer, done).wait_recv()
-                with scope(f"block_{layer}_{seg}"):
-                    results = scores(layer, seg)
-                    if seg == last - 1:
-                        own_half(hidden, layer, last)
-                    elif seg > 0:
-                        other_half(layer, done)
-                    else:
-                        own_half(hidden, layer, seg + 1)
-                    if seg == 0:
-                        with scope("halo_v"):
-                            wait_halo(layer, seg, 1)
-                    weigh(layer, seg, results)
-                    if 0 < seg < last - 1:
-                        finish(layer, done)
-                pair_copy(layer, seg).start()
-                if 0 < seg < last - 1:
-                    done = done - 1
-                    with scope(f"own_{layer}_{done}"):
-                        own_half(hidden, layer, done)
-                    if seg == 1:
-                        with scope(f"pair_{layer}_{done}"):
-                            pair_copy(layer, done).wait_recv()
-                        with scope(f"finish_{layer}_{done}"):
-                            other_half(layer, done)
-                            finish(layer, done)
-                        done = done - 1
-            while done >= 0:
-                if done == 0:
-                    with scope(f"own_{layer}_{done}"):
-                        own_half(hidden, layer, done)
-                with scope(f"pair_{layer}_{done}"):
-                    pair_copy(layer, done).wait_recv()
-                with scope(f"finish_{layer}_{done}"):
-                    other_half(layer, done)
-                    finish(layer, done)
-                done = done - 1
+                    weigh(layer, seg - 1, soften(results))
+                finish(layer, one(seg))
+            if seg > 0:
+                pair_copy(layer, seg - 1).start()
+            with scope(f"kv_{layer}_{seg}"):
+                keys_values(following, layer + 1, one(seg))
+            with scope(f"own_{layer}_{seg}"):
+                if seg > 0:
+                    own_half(hidden, layer, one(seg - 1))
+                queries_split(following, layer + 1, seg)
+
+    layer, hidden = LAYERS - 1, hiddens[LAYERS - 1]
+    late, late_piece = range(2, segments)[::-1], (2, segments)
+    with scope("halo_late"):
+        for seg in late:
+            wait_halo(layer, seg)
+    with scope("attend_late"):
+        results = [scores(layer, seg) for seg in late]
+        for seg, result in zip(late, results):
+            weigh(layer, seg, soften(result))
+    for seg in late:
+        pair_copy(layer, seg).start()
+    with scope("own_late"):
+        own_half(hidden, layer, late_piece)
+    with scope("halo_1"):
+        wait_halo(layer, 1)
+    with scope("pair_late"):
+        for seg in late:
+            pair_copy(layer, seg).wait_recv()
+    with scope("block_1_late"):
+        result = scores(layer, 1)
+        other_half(layer, late_piece)
+        weigh(layer, 1, soften(result))
+        finish(layer, late_piece)
+    pair_copy(layer, 1).start()
+    with scope("k_0"):
+        wait_halo(layer, 0, 0)
+    with scope("soften_0_own_1"):
+        result = scores(layer, 0)
+        own_half(hidden, layer, one(1))
+        softened = soften(result)
+    with scope("v_0"):
+        wait_halo(layer, 0, 1)
+    with scope("weigh_0"):
+        weigh(layer, 0, softened)
+    pair_copy(layer, 0).start()
+    with scope("pair_1"):
+        pair_copy(layer, 1).wait_recv()
+    with scope("finish_1"):
+        other_half(layer, one(1))
+        own_half(hidden, layer, one(0))
+        finish(layer, one(1))
+    with scope("pair_0"):
+        pair_copy(layer, 0).wait_recv()
+    with scope("finish_0"):
+        other_half(layer, one(0))
+        finish(layer, one(0))
 
     for layer in range(LAYERS):
         for seg in range(segments):
@@ -481,7 +501,7 @@
             pltpu.VMEM((LAYERS, reach + rows, width), bf16),
             pltpu.VMEM((LAYERS, rows, width), bf16),
             pltpu.VMEM((LAYERS, rows, width), bf16),
-            pltpu.VMEM((2, SEG, model), jnp.float32),
+            pltpu.VMEM((rows, model), jnp.float32),
             pltpu.VMEM((LAYERS, heads * SEG, wide), jnp.float32),
             pltpu.VMEM((-(-LAYERS * heads // 8) * 8, size), jnp.float32),
             pltpu.SemaphoreType.DMA((2,)),

time: 21.4 us -> 20.7 us (0.967)
  Pallas kernels: 20.5 us -> 19.8 us
    pallas_call x1, Pallas kernels: 20.5 us -> 19.8 us  [body(): pl.pallas_call(functools.partial(kernel, sp_count, heads), out_shape=jax....]
where the time goes in v3:
time: 20.7 us; the launch traced here: 20.6 us
  Pallas kernels  19.8 us (96%)
  local copies, waits for them, and re-layouts  0.8 us (4%)
    pallas_call x1, Pallas kernels, body(): pl.pallas_call(functools.partial(kernel, sp_count, heads), out_shape=jax....  19.8 us
    unnamed x1, local copies, waits for them, and re-layouts  0.8 us

profile of v3, /device:TPU:25, one launch (start us, length us, event | category | flops | bytes accessed | tf_op | source)
XLA Modules:
  0.0 20.6 jit_solution(5260847897579796236)
XLA Ops:
  0.0 19.8 %shard_map.82 = bf16[256,1024]{1,0:T(8,128)(2,1)S(1)} custom-call(bf16[256,2048]{1,0:T(8,128)(2,1)} %tokens.1, bf16[2,2048,256]{2,1,0:T(8,128)(2,1)} %wq_hbm.1, bf16[2,2048,256]{2,1,0:T(8,128)(2,1)} %wk_hbm.1, bf16[2,2048,256]{2,1,0:T(8,128)(2,1)} %wv_hbm.1, bf16[2,512,2048]{2,1,0:T(8,128)(2,1)} %wo_hbm.1, f32[2,4,257]{2,1,0:T(4,128)} %table_hbm.1, ...), custom_call_target="tpu_custom_call" | custom-call | tf_op jit(solution)/shard_map/pallas_call | solution.py:484
  19.8 0.8 %copy.10 = bf16[256,1024]{1,0:T(8,128)(2,1)} copy(bf16[256,1024]{1,0:T(8,128)(2,1)S(1)} %shard_map.82) | data formatting | bytes 1048576

commit v4 on v3

--- a/solution.py
+++ b/solution.py
@@ -185,7 +185,8 @@
         kx[layer, target, :] = project(hidden, layer, part, 0)
         vx[layer, target, :] = project(hidden, layer, part, 1)
 
-        @pl.when(has_next)
+    def send(layer, piece, core):
+        @pl.when(has_next & (tp == core))
         def _():
             for seg in range(*piece)[::-1]:
                 halo_copy(0, layer, seg).start()
@@ -353,11 +354,16 @@
         x_rest.wait()
     for copy in (*small, w_copy(3, 0), w_copy(4, 0)):
         copy.start()
+    with scope("kv_next"):
+        keys_values(x0, 0, (last - 1, last))
+        send(0, (last - 1, last), 0)
     with scope("kv_rest"):
-        keys_values(x0, 0, (0, last))
+        keys_values(x0, 0, (0, last - 1))
+        send(0, (0, last - 1), 0)
     w_copy(2, 0).wait()
     with scope("queries"):
         queries(x0, 0, (0, segments))
+    send(0, (0, last), 1)
     for kind in range(5):
         w_copy(kind, 1).start()
     for copy in small:
@@ -403,10 +409,12 @@
                 pair_copy(layer, seg - 1).start()
             with scope(f"kv_{layer}_{seg}"):
                 keys_values(following, layer + 1, one(seg))
+                send(layer + 1, one(seg), 0)
             with scope(f"own_{layer}_{seg}"):
                 if seg > 0:
                     own_half(hidden, layer, one(seg - 1))
                 queries_split(following, layer + 1, seg)
+                send(layer + 1, one(seg), 1)
 
     layer, hidden = LAYERS - 1, hiddens[LAYERS - 1]
     late, late_piece = range(2, segments)[::-1], (2, segments)

time: 20.7 us -> 20.6 us (level)
  no operation moved by 1% of the time
where the time goes in v4:
time: 20.6 us; the launch traced here: 20.4 us
  Pallas kernels  19.6 us (95%)
  local copies, waits for them, and re-layouts  0.8 us (4%)
    pallas_call x1, Pallas kernels, body(): pl.pallas_call(functools.partial(kernel, sp_count, heads), out_shape=jax....  19.6 us
    unnamed x1, local copies, waits for them, and re-layouts  0.8 us

profile of v4, /device:TPU:25, one launch (start us, length us, event | category | flops | bytes accessed | tf_op | source)
XLA Modules:
  0.0 20.4 jit_solution(5488246601967421153)
XLA Ops:
  0.0 19.6 %shard_map.82 = bf16[256,1024]{1,0:T(8,128)(2,1)S(1)} custom-call(bf16[256,2048]{1,0:T(8,128)(2,1)} %tokens.1, bf16[2,2048,256]{2,1,0:T(8,128)(2,1)} %wq_hbm.1, bf16[2,2048,256]{2,1,0:T(8,128)(2,1)} %wk_hbm.1, bf16[2,2048,256]{2,1,0:T(8,128)(2,1)} %wv_hbm.1, bf16[2,512,2048]{2,1,0:T(8,128)(2,1)} %wo_hbm.1, f32[2,4,257]{2,1,0:T(4,128)} %table_hbm.1, ...), custom_call_target="tpu_custom_call" | custom-call | tf_op jit(solution)/shard_map/pallas_call | solution.py:492
  19.6 0.8 %copy.10 = bf16[256,1024]{1,0:T(8,128)(2,1)} copy(bf16[256,1024]{1,0:T(8,128)(2,1)S(1)} %shard_map.82) | data formatting | bytes 1048576

commit v5 on v4

--- a/solution.py
+++ b/solution.py
@@ -361,15 +361,17 @@
         keys_values(x0, 0, (0, last - 1))
         send(0, (0, last - 1), 0)
     w_copy(2, 0).wait()
+    for kind in range(2):
+        w_copy(kind, 1).start()
     with scope("queries"):
         queries(x0, 0, (0, segments))
     send(0, (0, last), 1)
-    for kind in range(5):
-        w_copy(kind, 1).start()
     for copy in small:
         copy.wait()
     with scope("bias"):
         build_bias()
+    for kind in range(2, 5):
+        w_copy(kind, 1).start()
     w_copy(3, 0).wait()
     w_copy(4, 0).wait()
 
@@ -390,33 +392,42 @@
         pair_copy(layer, last).start()
         with scope(f"own_{layer}_{last}"):
             own_half(hidden, layer, one(last))
-        for kind in range(5):
-            w_copy(kind, layer + 1).wait()
         for seg in range(segments)[::-1]:
             if seg > 0:
                 with scope(f"halo_{layer}_{seg - 1}"):
                     wait_halo(layer, seg - 1)
             with scope(f"pair_{layer}_{seg}"):
                 pair_copy(layer, seg).wait_recv()
+            if seg == last:
+                with scope(f"w_{layer}"):
+                    for kind in range(3):
+                        w_copy(kind, layer + 1).wait()
             with scope(f"block_{layer}_{seg}"):
                 if seg > 0:
                     results = scores(layer, seg - 1)
                 other_half(layer, one(seg))
                 if seg > 0:
                     weigh(layer, seg - 1, soften(results))
-                finish(layer, one(seg))
             if seg > 0:
                 pair_copy(layer, seg - 1).start()
             with scope(f"kv_{layer}_{seg}"):
-                keys_values(following, layer + 1, one(seg))
-                send(layer + 1, one(seg), 0)
-            with scope(f"own_{layer}_{seg}"):
                 if seg > 0:
                     own_half(hidden, layer, one(seg - 1))
-                queries_split(following, layer + 1, seg)
-                send(layer + 1, one(seg), 1)
+                finish(layer, one(seg))
+                keys_values(following, layer + 1, one(seg))
+                if seg > 0:
+                    queries_split(following, layer + 1, seg)
+                send(layer + 1, one(seg), 0)
+                if seg > 0:
+                    send(layer + 1, one(seg), 1)
+            if seg == 0:
+                with scope(f"q_{layer}_{seg}"):
+                    queries_split(following, layer + 1, seg)
+                    send(layer + 1, one(seg), 1)
 
     layer, hidden = LAYERS - 1, hiddens[LAYERS - 1]
+    w_copy(3, layer).wait()
+    w_copy(4, layer).wait()
     late, late_piece = range(2, segments)[::-1], (2, segments)
     with scope("halo_late"):
         for seg in late:

time: 20.6 us -> 20 us (0.971)
  Pallas kernels: 19.6 us -> 19 us
    pallas_call x1, Pallas kernels: 19.6 us -> 19 us  [body(): pl.pallas_call(functools.partial(kernel, sp_count, heads), out_shape=jax....]
where the time goes in v5:
time: 20 us; the launch traced here: 19.8 us
  Pallas kernels  19 us (95%)
  local copies, waits for them, and re-layouts  0.8 us (4%)
    pallas_call x1, Pallas kernels, body(): pl.pallas_call(functools.partial(kernel, sp_count, heads), out_shape=jax....  19 us
    unnamed x1, local copies, waits for them, and re-layouts  0.8 us

profile of v5, /device:TPU:25, one launch (start us, length us, event | category | flops | bytes accessed | tf_op | source)
XLA Modules:
  0.0 19.8 jit_solution(17113101066684060241)
XLA Ops:
  0.0 19.0 %shard_map.82 = bf16[256,1024]{1,0:T(8,128)(2,1)S(1)} custom-call(bf16[256,2048]{1,0:T(8,128)(2,1)} %tokens.1, bf16[2,2048,256]{2,1,0:T(8,128)(2,1)} %wq_hbm.1, bf16[2,2048,256]{2,1,0:T(8,128)(2,1)} %wk_hbm.1, bf16[2,2048,256]{2,1,0:T(8,128)(2,1)} %wv_hbm.1, bf16[2,512,2048]{2,1,0:T(8,128)(2,1)} %wo_hbm.1, f32[2,4,257]{2,1,0:T(4,128)} %table_hbm.1, ...), custom_call_target="tpu_custom_call" | custom-call | tf_op jit(solution)/shard_map/pallas_call | solution.py:503
  19.0 0.8 %copy.10 = bf16[256,1024]{1,0:T(8,128)(2,1)} copy(bf16[256,1024]{1,0:T(8,128)(2,1)S(1)} %shard_map.82) | data formatting | bytes 1048576

commit v6 on v5

--- a/solution.py
+++ b/solution.py
@@ -415,15 +415,13 @@
                     own_half(hidden, layer, one(seg - 1))
                 finish(layer, one(seg))
                 keys_values(following, layer + 1, one(seg))
-                if seg > 0:
-                    queries_split(following, layer + 1, seg)
                 send(layer + 1, one(seg), 0)
                 if seg > 0:
                     send(layer + 1, one(seg), 1)
             if seg == 0:
                 with scope(f"q_{layer}_{seg}"):
-                    queries_split(following, layer + 1, seg)
                     send(layer + 1, one(seg), 1)
+                    queries(following, layer + 1, (2, segments))
 
     layer, hidden = LAYERS - 1, hiddens[LAYERS - 1]
     w_copy(3, layer).wait()
@@ -440,6 +438,7 @@
         pair_copy(layer, seg).start()
     with scope("own_late"):
         own_half(hidden, layer, late_piece)
+        queries(hidden, layer, (0, 2))
     with scope("halo_1"):
         wait_halo(layer, 1)
     with scope("pair_late"):

time: 20 us -> 19.9 us (level)
  no operation moved by 1% of the time
where the time goes in v6:
time: 19.9 us; the launch traced here: 19.7 us
  Pallas kernels  18.9 us (95%)
  local copies, waits for them, and re-layouts  0.8 us (4%)
    pallas_call x1, Pallas kernels, body(): pl.pallas_call(functools.partial(kernel, sp_count, heads), out_shape=jax....  18.9 us
    unnamed x1, local copies, waits for them, and re-layouts  0.8 us

profile of v6, /device:TPU:25, one launch (start us, length us, event | category | flops | bytes accessed | tf_op | source)
XLA Modules:
  0.0 19.7 jit_solution(8297414440608894284)
XLA Ops:
  0.0 18.9 %shard_map.82 = bf16[256,1024]{1,0:T(8,128)(2,1)S(1)} custom-call(bf16[256,2048]{1,0:T(8,128)(2,1)} %tokens.1, bf16[2,2048,256]{2,1,0:T(8,128)(2,1)} %wq_hbm.1, bf16[2,2048,256]{2,1,0:T(8,128)(2,1)} %wk_hbm.1, bf16[2,2048,256]{2,1,0:T(8,128)(2,1)} %wv_hbm.1, bf16[2,512,2048]{2,1,0:T(8,128)(2,1)} %wo_hbm.1, f32[2,4,257]{2,1,0:T(4,128)} %table_hbm.1, ...), custom_call_target="tpu_custom_call" | custom-call | tf_op jit(solution)/shard_map/pallas_call | solution.py:502
  18.9 0.8 %copy.10 = bf16[256,1024]{1,0:T(8,128)(2,1)} copy(bf16[256,1024]{1,0:T(8,128)(2,1)S(1)} %shard_map.82) | data formatting | bytes 1048576

commit v7 on v6

--- a/solution.py
+++ b/solution.py
@@ -135,7 +135,7 @@
     first = [first_copy(kind, index) for kind in range(2) for index in range(CHUNKS)]
     for copy in first[:CHUNKS]:
         copy.start()
-    pl.delay(200)
+    pl.delay(120)
     for copy in first[CHUNKS:]:
         copy.start()
     x_rest.start()
@@ -309,7 +309,7 @@
         total[rows_of(piece), :] += half(layer, piece, peer, 1)
 
     def finish(layer, piece):
-        step = 16
+        step = 8
         part = rows_of(piece)
         for r in range(part.start, part.stop, step):
             here = slice(r, r + step)

time: 19.9 us -> 19.8 us (level)
  no operation moved by 1% of the time
where the time goes in v7:
time: 19.8 us; the launch traced here: 19.7 us
  Pallas kernels  18.9 us (95%)
  local copies, waits for them, and re-layouts  0.8 us (4%)
    pallas_call x1, Pallas kernels, body(): pl.pallas_call(functools.partial(kernel, sp_count, heads), out_shape=jax....  18.9 us
    unnamed x1, local copies, waits for them, and re-layouts  0.8 us

profile of v7, /device:TPU:25, one launch (start us, length us, event | category | flops | bytes accessed | tf_op | source)
XLA Modules:
  0.0 19.7 jit_solution(9828722636403336715)
XLA Ops:
  0.0 18.9 %shard_map.82 = bf16[256,1024]{1,0:T(8,128)(2,1)S(1)} custom-call(bf16[256,2048]{1,0:T(8,128)(2,1)} %tokens.1, bf16[2,2048,256]{2,1,0:T(8,128)(2,1)} %wq_hbm.1, bf16[2,2048,256]{2,1,0:T(8,128)(2,1)} %wk_hbm.1, bf16[2,2048,256]{2,1,0:T(8,128)(2,1)} %wv_hbm.1, bf16[2,512,2048]{2,1,0:T(8,128)(2,1)} %wo_hbm.1, f32[2,4,257]{2,1,0:T(4,128)} %table_hbm.1, ...), custom_call_target="tpu_custom_call" | custom-call | tf_op jit(solution)/shard_map/pallas_call | solution.py:502
  18.9 0.8 %copy.10 = bf16[256,1024]{1,0:T(8,128)(2,1)} copy(bf16[256,1024]{1,0:T(8,128)(2,1)S(1)} %shard_map.82) | data formatting | bytes 1048576

commit v8 on v7

--- a/solution.py
+++ b/solution.py
@@ -365,11 +365,12 @@
         w_copy(kind, 1).start()
     with scope("queries"):
         queries(x0, 0, (0, segments))
-    send(0, (0, last), 1)
+    send(0, (last - 1, last), 1)
     for copy in small:
         copy.wait()
     with scope("bias"):
         build_bias()
+    send(0, (0, last - 1), 1)
     for kind in range(2, 5):
         w_copy(kind, 1).start()
     w_copy(3, 0).wait()

time: 19.8 us -> 19.8 us (level)
  no operation moved by 1% of the time
where the time goes in v8:
time: 19.8 us; the launch traced here: 19.7 us
  Pallas kernels  18.9 us (95%)
  local copies, waits for them, and re-layouts  0.8 us (4%)
    pallas_call x1, Pallas kernels, body(): pl.pallas_call(functools.partial(kernel, sp_count, heads), out_shape=jax....  18.9 us
    unnamed x1, local copies, waits for them, and re-layouts  0.8 us

profile of v8, /device:TPU:25, one launch (start us, length us, event | category | flops | bytes accessed | tf_op | source)
XLA Modules:
  0.0 19.7 jit_solution(5048653923409833292)
XLA Ops:
  0.0 18.9 %shard_map.82 = bf16[256,1024]{1,0:T(8,128)(2,1)S(1)} custom-call(bf16[256,2048]{1,0:T(8,128)(2,1)} %tokens.1, bf16[2,2048,256]{2,1,0:T(8,128)(2,1)} %wq_hbm.1, bf16[2,2048,256]{2,1,0:T(8,128)(2,1)} %wk_hbm.1, bf16[2,2048,256]{2,1,0:T(8,128)(2,1)} %wv_hbm.1, bf16[2,512,2048]{2,1,0:T(8,128)(2,1)} %wo_hbm.1, f32[2,4,257]{2,1,0:T(4,128)} %table_hbm.1, ...), custom_call_target="tpu_custom_call" | custom-call | tf_op jit(solution)/shard_map/pallas_call | solution.py:503
  18.9 0.8 %copy.10 = bf16[256,1024]{1,0:T(8,128)(2,1)} copy(bf16[256,1024]{1,0:T(8,128)(2,1)S(1)} %shard_map.82) | data formatting | bytes 1048576
